TPU v7x, 32 devices: a whole 2x2x4 slice. The times are simulated.
32 devices in a mesh: ep: 8 (over z, x), tp: 4 (over y, core).
Axes of the slice: x: 2, y: 2, z: 4, core: 2. Of those that a mesh axis runs over, the one named last changes fastest.
Arguments:
- mix_bgate: bfloat16 [2048, 1024], P('ep', 'tp'), may hold values from -6 to 6
- mix_cgate: bfloat16 [2048, 1024], P('ep', 'tp'), may hold values from -6 to 6
- mix_input: bfloat16 [2048, 1024], P('ep', 'tp'), may hold values from -6 to 6
- conv_taps: float32 [3, 1024], P(None, 'tp'), may hold values from -3.5 to 3.5
- mix_out_w: bfloat16 [1024, 2048], P('tp'), may hold values from -0.1875 to 0.1875
- moe_x: bfloat16 [2048, 2048], P('ep', 'tp'), may hold values from -6 to 6
- moe_gain: float32 [2048], replicated, may hold values from 0.1 to 1.9
- routes: int32 [2048, 2], P('ep'), may hold values from 0 to 7, all different within a row; in each aligned block of 256 rows (0 to 255, 256 to 511, ...) at most 96 rows name the same one
- route_w: float32 [2048, 2], P('ep'), may hold values from 0.2 to 1
- w_gate: bfloat16 [8, 2048, 3584], P('ep', None, 'tp'), may hold values from -0.125 to 0.125
- w_up: bfloat16 [8, 2048, 3584], P('ep', None, 'tp'), may hold values from -0.125 to 0.125
- w_down: bfloat16 [8, 3584, 2048], P('ep', 'tp'), may hold values from -0.09375 to 0.09375
Outputs:
- mixed: bfloat16 [2048, 2048], P(('ep', 'tp'))
- routed: bfloat16 [2048, 2048], P('ep', 'tp')
Inputs may be any that keep to these rules, and one draw needn't show every extreme that they name: `routes`: among the 256 rows of one index of ep, each row names 2 different experts and no expert is named by more than 96 rows; in every draw some expert is named by exactly 96 rows of some index.
All inputs are finite; a program needn't handle non-finite values.
Results may differ from a plain program's by a relative error of at most 0.012.
Values may be sent and summed in bfloat16 or wider, within the bound.
A program may use at most 64 MiB of HBM per device.

v0:
```python
import jax
import jax.numpy as jnp
from jax import lax
from jax.sharding import PartitionSpec as P


def shifted(block, axis, distance):
    devices = range(lax.axis_size(axis))
    route = [(i - distance, i) for i in devices if i - distance in devices]
    return lax.ppermute(block, axis, route)


def rms_rows(values, gain):
    wide = values.astype(jnp.float32)
    scale = lax.rsqrt(jnp.mean(wide * wide, axis=-1, keepdims=True) + 1e-06)
    return (wide * scale * gain).astype(jnp.bfloat16)


def conv_mixer(mix_bgate, mix_cgate, mix_input, conv_taps, mix_out_w):
    length = mix_input.shape[0]
    reach = conv_taps.shape[0] - 1
    tail = jnp.stack([mix_cgate[length - reach :], mix_input[length - reach :]])
    before = shifted(tail, "ep", 1)
    gates_c = jnp.concatenate([before[0], mix_cgate], 0).astype(jnp.float32)
    inputs_h = jnp.concatenate([before[1], mix_input], 0).astype(jnp.float32)
    prod = gates_c * inputs_h
    conv = conv_taps[0] * prod[0:length]
    for j in range(1, reach + 1):
        conv = conv + conv_taps[j] * prod[j : j + length]
    gated = (mix_bgate.astype(jnp.float32) * conv).astype(jnp.bfloat16)
    return lax.psum_scatter(
        jnp.dot(gated, mix_out_w, preferred_element_type=jnp.float32).astype(jnp.bfloat16),
        "tp",
        scatter_dimension=0,
        tiled=True,
    )


def expert_layer(moe_x, moe_gain, routes, route_w, w_gate, w_up, w_down):
    whole = lax.all_gather(moe_x, "tp", axis=1, tiled=True)
    normed = rms_rows(whole, moe_gain)
    ntok, width = normed.shape
    top = routes.shape[1]
    n_ep = lax.axis_size("ep")
    n_tp = lax.axis_size("tp")
    per_dev = w_gate.shape[0]
    experts = per_dev * n_ep
    cap = 4 * ((3 * ntok * top + 8 * experts - 1) // (8 * experts))
    flat = routes.reshape(-1)
    onehot = (flat[:, None] == jnp.arange(experts, dtype=jnp.int32)[None, :]).astype(jnp.int32)
    earlier = jnp.cumsum(onehot, axis=0) - onehot
    slot = jnp.sum(earlier * onehot, axis=1)
    place = flat * cap + slot
    source = (
        jnp.full((experts * cap,), ntok, jnp.int32)
        .at[place]
        .set(jnp.arange(ntok * top, dtype=jnp.int32) // top)
    )
    padded = jnp.concatenate([normed, jnp.zeros((1, width), jnp.bfloat16)], 0)
    outgoing = padded[source].reshape(n_ep, per_dev, cap, width)
    part = cap // n_tp
    mine = lax.dynamic_slice_in_dim(outgoing, lax.axis_index("tp") * part, part, 2)
    landed = lax.all_to_all(mine, "ep", split_axis=0, concat_axis=0, tiled=True)
    arrived = lax.all_gather(landed, "tp", axis=2, tiled=True)
    gate = jnp.einsum("secd,edf->secf", arrived, w_gate, preferred_element_type=jnp.float32)
    upper = jnp.einsum("secd,edf->secf", arrived, w_up, preferred_element_type=jnp.float32)
    hidden = (jax.nn.silu(gate) * upper).astype(jnp.bfloat16)
    down = jnp.einsum("secf,efd->secd", hidden, w_down, preferred_element_type=jnp.float32)
    summed = lax.psum_scatter(down.astype(jnp.bfloat16), "tp", scatter_dimension=3, tiled=True)
    returned = lax.all_to_all(summed, "ep", split_axis=0, concat_axis=0, tiled=True)
    flat_back = returned.reshape(experts * cap, width // n_tp)
    picked = flat_back[place].astype(jnp.float32).reshape(ntok, top, width // n_tp)
    return jnp.sum(picked * route_w[:, :, None], axis=1).astype(jnp.bfloat16)


def body(
    mix_bgate,
    mix_cgate,
    mix_input,
    conv_taps,
    mix_out_w,
    moe_x,
    moe_gain,
    routes,
    route_w,
    w_gate,
    w_up,
    w_down,
):
    mixed = conv_mixer(mix_bgate, mix_cgate, mix_input, conv_taps, mix_out_w)
    routed = expert_layer(moe_x, moe_gain, routes, route_w, w_gate, w_up, w_down)
    return (mixed, routed)


def solution(mesh):
    in_specs = (
        P("ep", "tp"),
        P("ep", "tp"),
        P("ep", "tp"),
        P(None, "tp"),
        P("tp", None),
        P("ep", "tp"),
        P(),
        P("ep", None),
        P("ep", None),
        P("ep", None, "tp"),
        P("ep", None, "tp"),
        P("ep", "tp", None),
    )
    out_specs = (P(("ep", "tp"), None), P("ep", "tp"))
    return jax.shard_map(body, mesh=mesh, in_specs=in_specs, out_specs=out_specs, check_vma=False)
```

profile of v0, /device:TPU:0, one launch (start us, length us, event | category | flops | bytes accessed | tf_op | source)
XLA Modules:
  0.0 185.2 jit_solution(3375936974495529147)
XLA Ops:
  7.2 0.0 copy-start
  7.2 0.0 all-gather.3.cloned.1.call-start
  7.2 0.7 all-gather.3.cloned.1.call-update
  7.9 0.0 all-gather.5.cloned.1.call-start
  8.0 0.8 copy.20
  8.8 0.1 eq.29
  8.9 0.1 eq.25
  9.1 1.1 reduce-window.6
  10.2 0.2 slice_reduce_fusion
  10.5 0.7 broadcast_multiply_fusion
  11.2 0.1 copy.19
  11.3 0.1 mul.110
  11.5 0.1 fusion.43
  11.6 2.4 %scatter_custom_fusion = s32[768]{0:T(1024)S(1)} fusion(s32[512]{0:T(512)S(1)} %bitcast.108, s32[512]{0:T(512)S(1)} %add_select_fusion, s32[]{:T(128)} %constant.40.clone.1), kind=kCustom, calls=%fused_computation.57 | custom fusion | bytes 3076 | tf_op jit(solution)/shard_map/scatter | solution.py:57
  14.1 15.0 %all-gather.3.cloned.1.call-done = bf16[256,2048]{1,0:T(8,128)(2,1)} async-done(((bf16[256,512]{1,0:T(8,128)(2,1)}), bf16[256,2048]{1,0:T(8,128)(2,1)}) %all-gather.3.cloned.1.call-update) | async-done | bytes 1048592 | tf_op jit(solution)/shard_map/all_gather | solution.py:40
  29.0 1.5 fusion.18
  30.6 1.5 fusion.20
  32.1 0.1 concatenate.11
  32.2 4.3 %gather_fusion = bf16[768,2048]{1,0:T(8,128)(2,1)} fusion(bf16[257,2048]{1,0:T(8,128)(2,1)S(1)} %concatenate.11, s32[1024]{0:T(1024)S(1)} %pad_clamp_fusion.1), kind=kCustom, calls=%fused_computation | custom fusion | bytes 6294528 | tf_op jit(solution)/shard_map/gather | solution.py:60
  36.5 1.2 constant_dynamic-slice_fusion
  37.7 25.9 %all_to_all.10 = bf16[8,1,24,2048]{3,2,1,0:T(8,128)(2,1)} all-to-all(bf16[8,1,24,2048]{3,2,1,0:T(8,128)(2,1)S(1)} %constant_dynamic-slice_fusion), channel_id=1, replica_groups=mesh['ep'=8,'tp'=4] {'ep'}, dimensions={0} | all-to-all | bytes 1572864 | tf_op jit(solution)/shard_map/all_to_all | solution.py:63
  63.6 0.0 all-gather.5.cloned.1.call-update
  63.6 0.0 reduce-scatter.5.cloned.1.call-start
  63.7 26.7 %all-gather.5.cloned.1.call-done = bf16[8,1,96,2048]{3,2,0,1:T(8,128)(2,1)} async-done(((bf16[8,1,24,2048]{3,2,0,1:T(8,128)(2,1)}), bf16[8,1,96,2048]{3,2,0,1:T(8,128)(2,1)}) %all-gather.5.cloned.1.call-update) | async-done | bytes 3145744 | tf_op jit(solution)/shard_map/all_gather | solution.py:64
  90.4 8.0 %fusion.4 = f32[8,96,896]{2,1,0:T(8,128)} fusion(bf16[1,2048,896]{2,1,0:T(8,128)(2,1)} %param.21, bf16[8,1,96,2048]{3,2,0,1:T(8,128)(2,1)} %all-gather.5.cloned.1.call-done), kind=kOutput, calls=%fused_computation.7 | convolution fusion | flops 2818572288 | bytes 9568256 | tf_op jit(solution)/shard_map/secd,edf->secf/dot_general | solution.py:65
  98.4 12.1 %fusion.11 = bf16[8,1,96,2048]{3,2,0,1:T(8,128)(2,1)} fusion(bf16[1,896,2048]{2,1,0:T(8,128)(2,1)} %param.23, bf16[1,2048,896]{2,1,0:T(8,128)(2,1)} %param.22, bf16[8,1,96,2048]{3,2,0,1:T(8,128)(2,1)} %all-gather.5.cloned.1.call-done, f32[8,96,896]{2,1,0:T(8,128)} %fusion.4), kind=kOutput, calls=%fused_computation.12 | convolution fusion | flops 5642846208 | bytes 16384000 | tf_op jit(solution)/shard_map/secf,efd->secd/dot_general | solution.py:68
  110.5 0.0 copy-start.1
  110.5 0.0 copy-start.2
  110.5 0.0 copy-start.4
  110.5 0.0 copy-start.3
  110.5 0.0 reduce-scatter.5.cloned.1.call-update
  110.5 0.0 copy-start.5
  110.5 0.0 reduce-scatter.3.cloned.1.call-start
  110.6 0.8 copy-done.1
  111.4 0.1 copy-done.2
  111.5 3.4 %collective-permute-start = (bf16[2,2,256]{2,1,0:T(2,128)(2,1)S(1)}, bf16[2,2,256]{2,1,0:T(2,128)(2,1)S(1)}, u32[]{:S(2)}, u32[]{:S(2)}) collective-permute-start(bf16[2,2,256]{2,1,0:T(2,128)(2,1)S(1)} %pad_maximum_fusion), channel_id=1, source_target_pairs={{0,4},{4,8},{8,12},{12,16},{16,20},{20,24},{24,28},{1,5},{5,9},{9,... | collective-permute-start | bytes 6152 | tf_op jit(solution)/shard_map/ppermute | solution.py:10
  114.9 0.0 copy-done.4
  114.9 1.3 collective-permute-done
  116.2 0.1 convert_multiply_fusion.2
  116.2 0.0 copy-done
  116.2 0.0 copy-done.3
  116.2 1.5 convolution_convert_fusion
  117.7 0.0 reduce-scatter.3.cloned.1.call-update
  117.7 30.7 %reduce-scatter.5.cloned.1.call-done = bf16[8,1,96,512]{3,2,0,1:T(8,128)(2,1)} async-done(((bf16[8,1,96,2048]{3,2,0,1:T(8,128)(2,1)}), bf16[8,1,96,512]{3,2,0,1:T(8,128)(2,1)}) %reduce-scatter.5.cloned.1.call-update) | async-done | bytes 786448 | tf_op jit(solution)/shard_map/reduce_scatter | solution.py:69
  148.4 5.5 %all-to-all-start.1 = ((bf16[8,1,96,512]{3,2,1,0:T(8,128)(2,1)}), bf16[8,1,96,512]{3,2,1,0:T(8,128)(2,1)S(1)}, u32[]{:S(2)}, u32[]{:S(2)}) async-start(bf16[8,1,96,512]{3,2,1,0:T(8,128)(2,1)} %bitcast.107), calls=%async_computation.3 | async-start | bytes 1572864 | tf_op jit(solution)/shard_map/all_to_all | solution.py:70
  153.9 0.0 copy-done.5
  153.9 0.1 copy.25
  154.1 19.9 %all-to-all-done.1 = bf16[8,1,96,512]{3,2,1,0:T(8,128)(2,1)S(1)} async-done(((bf16[8,1,96,512]{3,2,1,0:T(8,128)(2,1)}), bf16[8,1,96,512]{3,2,1,0:T(8,128)(2,1)S(1)}, u32[]{:S(2)}, u32[]{:S(2)}) %all-to-all-start.1) | async-done | bytes 786464 | tf_op jit(solution)/shard_map/all_to_all | solution.py:70
  174.0 2.0 %gather_fusion.1 = bf16[512,512]{1,0:T(8,128)(2,1)S(1)} fusion(bf16[768,512]{1,0:T(8,128)(2,1)S(1)} %bitcast.104, s32[1024]{0:T(1024)S(1)} %pad_clamp_fusion), kind=kCustom, calls=%fused_computation.1 | custom fusion | bytes 1050624 | tf_op jit(solution)/shard_map/gather | solution.py:72
  176.0 0.7 reshape.98
  176.6 2.1 %multiply_reduce_fusion = bf16[256,512]{1,0:T(8,128)(2,1)} fusion(f32[256,2,512]{2,1,0:T(2,128)S(1)} %reshape.98, f32[256,2]{1,0:T(8,128)S(1)} %copy.25), kind=kLoop, calls=%fused_computation.27 | loop fusion | flops 393216 | bytes 1312768 | tf_op jit(solution)/shard_map/reduce_sum | solution.py:73
  178.7 0.0 reduce-scatter.3.cloned.1.call-done
  (13 shorter events, 0.1 us)
Async XLA Ops:
  7.2 109.1 %copy-start = (bf16[256,2048]{1,0:T(8,128)(2,1)S(1)}, bf16[256,2048]{1,0:T(8,128)(2,1)}, u32[]{:S(2)}) copy-start(bf16[256,2048]{1,0:T(8,128)(2,1)} %param.16) | copy-start | bytes 3145732
  7.2 21.9 %all-gather.3.cloned.1.call-start = ((), (), s32[]{:S(2)}) async-start(), calls=%async_computation.5 | async-start | bytes 1310720 | tf_op jit(solution)/shard_map/all_gather | solution.py:40
  7.9 82.5 %all-gather.5.cloned.1.call-start = ((), (), s32[]{:S(2)}) async-start(), calls=%async_computation.6 | async-start | bytes 3932160 | tf_op jit(solution)/shard_map/all_gather | solution.py:64
  63.6 84.8 %reduce-scatter.5.cloned.1.call-start = ((), (), s32[]{:S(2)}) async-start(), calls=%async_computation.7 | async-start | bytes 3932160 | tf_op jit(solution)/shard_map/reduce_scatter | solution.py:69
  110.5 0.9 copy-start.1
  110.5 1.0 copy-start.2
  110.5 4.4 %copy-start.4 = (f32[3,256]{1,0:T(4,128)S(1)}, f32[3,256]{1,0:T(4,128)}, u32[]{:S(2)}) copy-start(f32[3,256]{1,0:T(4,128)} %param.15) | copy-start | bytes 9220
  110.5 5.7 %copy-start.3 = (bf16[256,256]{1,0:T(8,128)(2,1)S(1)}, bf16[256,256]{1,0:T(8,128)(2,1)}, u32[]{:S(2)}) copy-start(bf16[256,256]{1,0:T(8,128)(2,1)} %param.12) | copy-start | bytes 393220
  110.5 43.4 %copy-start.5 = (f32[256,2]{0,1:T(2,128)S(1)}, f32[256,2]{0,1:T(2,128)}, u32[]{:S(2)}) copy-start(f32[256,2]{0,1:T(2,128)} %param.20) | copy-start | bytes 6148
  110.5 68.1 %reduce-scatter.3.cloned.1.call-start = ((), (), s32[]{:S(2)}) async-start(), calls=%async_computation.4 | async-start | bytes 1310720 | tf_op jit(solution)/shard_map/reduce_scatter | solution.py:31
  111.5 4.7 %collective-permute-start = (bf16[2,2,256]{2,1,0:T(2,128)(2,1)S(1)}, bf16[2,2,256]{2,1,0:T(2,128)(2,1)S(1)}, u32[]{:S(2)}, u32[]{:S(2)}) collective-permute-start(bf16[2,2,256]{2,1,0:T(2,128)(2,1)S(1)} %pad_maximum_fusion), channel_id=1, source_target_pairs={{0,4},{4,8},{8,12},{12,16},{16,20},{20,24},{24,28},{1,5},{5,9},{9,... | collective-permute-start | bytes 6152 | tf_op jit(solution)/shard_map/ppermute | solution.py:10
  148.4 25.6 %all-to-all-start.1 = ((bf16[8,1,96,512]{3,2,1,0:T(8,128)(2,1)}), bf16[8,1,96,512]{3,2,1,0:T(8,128)(2,1)S(1)}, u32[]{:S(2)}, u32[]{:S(2)}) async-start(bf16[8,1,96,512]{3,2,1,0:T(8,128)(2,1)} %bitcast.107), calls=%async_computation.3 | async-start | bytes 1572864 | tf_op jit(solution)/shard_map/all_to_all | solution.py:70
Sparse Core Ops, SparseCore 0:
  9.5 19.4 all-gather.2
  63.7 26.6 all-gather.4
  110.7 37.7 reduce-scatter.4
  151.4 24.7 reduce-scatter.2
where the time goes:
time: 186 us; the launch traced here: 185 us
  waiting for transfers between devices  94.3 us (51%)
  blocking collectives  25.9 us (14%)
  matrix products  21.5 us (12%)
  between operations  14 us (8%)
  local copies, waits for them, and re-layouts  13.3 us (7%)
  starting transfers between devices  9.05 us (5%)
  other arithmetic  7.18 us (4%)
    reduce_scatter x1, waiting for transfers between devices, expert_layer(): lax.psum_scatter(down.astype(jnp.bfloat16), 'tp', scatter_dimension=3, ti...  30.7 us
    all_gather x1, waiting for transfers between devices, expert_layer(): arrived = lax.all_gather(landed, 'tp', axis=2, tiled=True)  26.7 us
    all_to_all x1, blocking collectives, expert_layer(): landed = lax.all_to_all(mine, 'ep', split_axis=0, concat_axis=0, tiled=True)  25.9 us
    all_to_all x1, waiting for transfers between devices, expert_layer(): lax.all_to_all(summed, 'ep', split_axis=0, concat_axis=0, tiled=True)  19.9 us
    all_gather x1, waiting for transfers between devices, expert_layer(): whole = lax.all_gather(moe_x, 'tp', axis=1, tiled=True)  15 us
    dot_general x1, matrix products, expert_layer(): jnp.einsum('secf,efd->secd', hidden, w_down, preferred_element_type=jnp.f...  12.1 us
    dot_general x1, matrix products, expert_layer(): jnp.einsum('secd,edf->secf', arrived, w_gate, preferred_element_type=jnp....  8 us
    all_to_all x1, starting transfers between devices, expert_layer(): lax.all_to_all(summed, 'ep', split_axis=0, concat_axis=0, tiled=True)  5.52 us
  transfers between devices with their start and end apart: 6, of which 5 were waited for; matrix products, arithmetic and copies ran while one was open for 7% of the time, Pallas kernels for 0%

commit v1 on v0

--- a/solution.py
+++ b/solution.py
@@ -37,7 +37,8 @@
 
 
 def expert_layer(moe_x, moe_gain, routes, route_w, w_gate, w_up, w_down):
-    whole = lax.all_gather(moe_x, "tp", axis=1, tiled=True)
+    shards = lax.all_gather(moe_x, "tp")
+    whole = jnp.concatenate(shards, axis=1)
     normed = rms_rows(whole, moe_gain)
     ntok, width = normed.shape
     top = routes.shape[1]

time: 186 us -> 187 us (level)
  local copies, waits for them, and re-layouts: 13.3 us -> 15.8 us
where the time goes in v1:
time: 187 us
  waiting for transfers between devices  94.3 us (50%)
  blocking collectives  25.9 us (14%)
  matrix products  21.5 us (11%)
  local copies, waits for them, and re-layouts  15.8 us (8%)
  between operations  14 us (7%)
  starting transfers between devices  9.05 us (5%)
  other arithmetic  6.17 us (3%)
    reduce_scatter x1, waiting for transfers between devices, expert_layer(): lax.psum_scatter(down.astype(jnp.bfloat16), 'tp', scatter_dimension=3, ti...  30.7 us
    all_gather x1, waiting for transfers between devices, expert_layer(): arrived = lax.all_gather(landed, 'tp', axis=2, tiled=True)  26.7 us
    all_to_all x1, blocking collectives, expert_layer(): landed = lax.all_to_all(mine, 'ep', split_axis=0, concat_axis=0, tiled=True)  25.9 us
    all_to_all x1, waiting for transfers between devices, expert_layer(): lax.all_to_all(summed, 'ep', split_axis=0, concat_axis=0, tiled=True)  19.9 us
    all_gather x1, waiting for transfers between devices, expert_layer(): shards = lax.all_gather(moe_x, 'tp')  15 us
    dot_general x1, matrix products, expert_layer(): jnp.einsum('secf,efd->secd', hidden, w_down, preferred_element_type=jnp.f...  12.1 us
    dot_general x1, matrix products, expert_layer(): jnp.einsum('secd,edf->secf', arrived, w_gate, preferred_element_type=jnp....  7.99 us
    all_to_all x1, starting transfers between devices, expert_layer(): lax.all_to_all(summed, 'ep', split_axis=0, concat_axis=0, tiled=True)  5.51 us
  transfers between devices with their start and end apart: 6, of which 5 were waited for; matrix products, arithmetic and copies ran while one was open for 7% of the time, Pallas kernels for 0%

profile of v1, /device:TPU:0, one launch (start us, length us, event | category | flops | bytes accessed | tf_op | source)
XLA Modules:
  0.0 186.8 jit_solution(10500130976953642716)
XLA Ops:
  7.2 0.0 copy-start
  7.2 0.0 all-gather.6.cloned.1.call-start
  7.2 0.7 all-gather.6.cloned.1.call-update
  7.9 0.0 all-gather.4.cloned.1.call-start
  8.0 0.8 copy.23
  8.8 0.1 eq.29
  8.9 0.1 eq.25
  9.1 1.1 reduce-window.6
  10.2 0.2 slice_reduce_fusion
  10.5 0.7 broadcast_multiply_fusion
  11.2 0.1 copy.22
  11.3 0.1 mul.112
  11.5 0.1 fusion.40
  11.6 2.4 %scatter_custom_fusion = s32[768]{0:T(1024)S(1)} fusion(s32[512]{0:T(512)S(1)} %bitcast.117, s32[512]{0:T(512)S(1)} %add_select_fusion, s32[]{:T(128)} %constant.40.clone.1), kind=kCustom, calls=%fused_computation.54 | custom fusion | bytes 3076 | tf_op jit(solution)/shard_map/scatter | solution.py:58
  14.1 15.0 %all-gather.6.cloned.1.call-done = bf16[1024,512]{1,0:T(8,128)(2,1)} async-done(((bf16[256,512]{1,0:T(8,128)(2,1)}), bf16[1024,512]{1,0:T(8,128)(2,1)}) %all-gather.6.cloned.1.call-update) | async-done | bytes 1048592 | tf_op jit(solution)/shard_map/all_gather | solution.py:40
  29.0 1.5 bitcast_convert_fusion
  30.6 1.4 copy.21
  31.9 0.0 copy-start.1
  31.9 0.0 copy-start.5
  31.9 0.9 copy.29
  32.8 0.3 copy-done.1
  33.1 0.3 multiply_reduce_fusion
  33.4 0.0 copy-done.5
  33.4 0.2 multiply_convert_fusion
  33.7 0.1 concatenate.11
  33.8 4.3 %gather_fusion = bf16[768,2048]{1,0:T(8,128)(2,1)} fusion(bf16[257,2048]{1,0:T(8,128)(2,1)S(1)} %concatenate.11, s32[1024]{0:T(1024)S(1)} %pad_clamp_fusion.1), kind=kCustom, calls=%fused_computation | custom fusion | bytes 6294528 | tf_op jit(solution)/shard_map/gather | solution.py:61
  38.1 1.2 constant_dynamic-slice_fusion
  39.3 25.9 %all_to_all.10 = bf16[8,1,24,2048]{3,2,1,0:T(8,128)(2,1)} all-to-all(bf16[8,1,24,2048]{3,2,1,0:T(8,128)(2,1)S(1)} %constant_dynamic-slice_fusion), channel_id=1, replica_groups=mesh['ep'=8,'tp'=4] {'ep'}, dimensions={0} | all-to-all | bytes 1572864 | tf_op jit(solution)/shard_map/all_to_all | solution.py:64
  65.2 0.0 all-gather.4.cloned.1.call-update
  65.2 0.0 reduce-scatter.5.cloned.1.call-start
  65.3 26.7 %all-gather.4.cloned.1.call-done = bf16[8,1,96,2048]{3,2,0,1:T(8,128)(2,1)} async-done(((bf16[8,1,24,2048]{3,2,0,1:T(8,128)(2,1)}), bf16[8,1,96,2048]{3,2,0,1:T(8,128)(2,1)}) %all-gather.4.cloned.1.call-update) | async-done | bytes 3145744 | tf_op jit(solution)/shard_map/all_gather | solution.py:65
  92.0 8.0 %fusion.4 = f32[8,96,896]{2,1,0:T(8,128)} fusion(bf16[1,2048,896]{2,1,0:T(8,128)(2,1)} %param.21, bf16[8,1,96,2048]{3,2,0,1:T(8,128)(2,1)} %all-gather.4.cloned.1.call-done), kind=kOutput, calls=%fused_computation.7 | convolution fusion | flops 2818572288 | bytes 9568256 | tf_op jit(solution)/shard_map/secd,edf->secf/dot_general | solution.py:66
  100.0 12.1 %fusion.11 = bf16[8,1,96,2048]{3,2,0,1:T(8,128)(2,1)} fusion(bf16[1,896,2048]{2,1,0:T(8,128)(2,1)} %param.23, bf16[1,2048,896]{2,1,0:T(8,128)(2,1)} %param.22, bf16[8,1,96,2048]{3,2,0,1:T(8,128)(2,1)} %all-gather.4.cloned.1.call-done, f32[8,96,896]{2,1,0:T(8,128)} %fusion.4), kind=kOutput, calls=%fused_computation.12 | convolution fusion | flops 5642846208 | bytes 16384000 | tf_op jit(solution)/shard_map/secf,efd->secd/dot_general | solution.py:69
  112.1 0.0 copy-start.2
  112.1 0.0 copy-start.3
  112.1 0.0 copy-start.6
  112.1 0.0 copy-start.4
  112.1 0.0 reduce-scatter.5.cloned.1.call-update
  112.1 0.0 copy-start.7
  112.1 0.0 reduce-scatter.3.cloned.1.call-start
  112.2 0.8 copy-done.2
  113.0 0.1 copy-done.3
  113.1 3.4 %collective-permute-start = (bf16[2,2,256]{2,1,0:T(2,128)(2,1)S(1)}, bf16[2,2,256]{2,1,0:T(2,128)(2,1)S(1)}, u32[]{:S(2)}, u32[]{:S(2)}) collective-permute-start(bf16[2,2,256]{2,1,0:T(2,128)(2,1)S(1)} %pad_maximum_fusion), channel_id=1, source_target_pairs={{0,4},{4,8},{8,12},{12,16},{16,20},{20,24},{24,28},{1,5},{5,9},{9,... | collective-permute-start | bytes 6152 | tf_op jit(solution)/shard_map/ppermute | solution.py:10
  116.5 0.0 copy-done.6
  116.5 1.3 collective-permute-done
  117.8 0.1 convert_multiply_fusion
  117.8 0.0 copy-done
  117.8 0.0 copy-done.4
  117.8 1.5 convolution_convert_fusion
  119.3 0.0 reduce-scatter.3.cloned.1.call-update
  119.3 30.7 %reduce-scatter.5.cloned.1.call-done = bf16[8,1,96,512]{3,2,0,1:T(8,128)(2,1)} async-done(((bf16[8,1,96,2048]{3,2,0,1:T(8,128)(2,1)}), bf16[8,1,96,512]{3,2,0,1:T(8,128)(2,1)}) %reduce-scatter.5.cloned.1.call-update) | async-done | bytes 786448 | tf_op jit(solution)/shard_map/reduce_scatter | solution.py:70
  150.0 5.5 %all-to-all-start.1 = ((bf16[8,1,96,512]{3,2,1,0:T(8,128)(2,1)}), bf16[8,1,96,512]{3,2,1,0:T(8,128)(2,1)S(1)}, u32[]{:S(2)}, u32[]{:S(2)}) async-start(bf16[8,1,96,512]{3,2,1,0:T(8,128)(2,1)} %bitcast.116), calls=%async_computation.3 | async-start | bytes 1572864 | tf_op jit(solution)/shard_map/all_to_all | solution.py:71
  155.5 0.0 copy-done.7
  155.5 0.1 copy.28
  155.7 19.9 %all-to-all-done.1 = bf16[8,1,96,512]{3,2,1,0:T(8,128)(2,1)S(1)} async-done(((bf16[8,1,96,512]{3,2,1,0:T(8,128)(2,1)}), bf16[8,1,96,512]{3,2,1,0:T(8,128)(2,1)S(1)}, u32[]{:S(2)}, u32[]{:S(2)}) %all-to-all-start.1) | async-done | bytes 786464 | tf_op jit(solution)/shard_map/all_to_all | solution.py:71
  175.6 2.0 %gather_fusion.1 = bf16[512,512]{1,0:T(8,128)(2,1)S(1)} fusion(bf16[768,512]{1,0:T(8,128)(2,1)S(1)} %bitcast.110, s32[1024]{0:T(1024)S(1)} %pad_clamp_fusion), kind=kCustom, calls=%fused_computation.1 | custom fusion | bytes 1050624 | tf_op jit(solution)/shard_map/gather | solution.py:73
  177.6 0.7 reshape.103
  178.2 2.1 %multiply_reduce_fusion.1 = bf16[256,512]{1,0:T(8,128)(2,1)} fusion(f32[256,2,512]{2,1,0:T(2,128)S(1)} %reshape.103, f32[256,2]{1,0:T(8,128)S(1)} %copy.28), kind=kLoop, calls=%fused_computation.24 | loop fusion | flops 393216 | bytes 1312768 | tf_op jit(solution)/shard_map/reduce_sum | solution.py:74
  180.3 0.0 reduce-scatter.3.cloned.1.call-done
  (13 shorter events, 0.1 us)
Async XLA Ops:
  7.2 110.7 %copy-start = (bf16[256,2048]{1,0:T(8,128)(2,1)S(1)}, bf16[256,2048]{1,0:T(8,128)(2,1)}, u32[]{:S(2)}) copy-start(bf16[256,2048]{1,0:T(8,128)(2,1)} %param.16) | copy-start | bytes 3145732
  7.2 21.9 %all-gather.6.cloned.1.call-start = ((), (), s32[]{:S(2)}) async-start(), calls=%async_computation.7 | async-start | bytes 1310720 | tf_op jit(solution)/shard_map/all_gather | solution.py:40
  7.9 84.1 %all-gather.4.cloned.1.call-start = ((), (), s32[]{:S(2)}) async-start(), calls=%async_computation.5 | async-start | bytes 3932160 | tf_op jit(solution)/shard_map/all_gather | solution.py:65
  31.9 1.2 copy-start.1
  31.9 1.5 copy-start.5
  65.2 84.8 %reduce-scatter.5.cloned.1.call-start = ((), (), s32[]{:S(2)}) async-start(), calls=%async_computation.6 | async-start | bytes 3932160 | tf_op jit(solution)/shard_map/reduce_scatter | solution.py:70
  112.1 0.9 copy-start.2
  112.1 1.0 copy-start.3
  112.1 4.4 %copy-start.6 = (f32[3,256]{1,0:T(4,128)S(1)}, f32[3,256]{1,0:T(4,128)}, u32[]{:S(2)}) copy-start(f32[3,256]{1,0:T(4,128)} %param.15) | copy-start | bytes 9220
  112.1 5.7 %copy-start.4 = (bf16[256,256]{1,0:T(8,128)(2,1)S(1)}, bf16[256,256]{1,0:T(8,128)(2,1)}, u32[]{:S(2)}) copy-start(bf16[256,256]{1,0:T(8,128)(2,1)} %param.12) | copy-start | bytes 393220
  112.1 43.4 %copy-start.7 = (f32[256,2]{0,1:T(2,128)S(1)}, f32[256,2]{0,1:T(2,128)}, u32[]{:S(2)}) copy-start(f32[256,2]{0,1:T(2,128)} %param.20) | copy-start | bytes 6148
  112.1 68.1 %reduce-scatter.3.cloned.1.call-start = ((), (), s32[]{:S(2)}) async-start(), calls=%async_computation.4 | async-start | bytes 1310720 | tf_op jit(solution)/shard_map/reduce_scatter | solution.py:31
  113.1 4.7 %collective-permute-start = (bf16[2,2,256]{2,1,0:T(2,128)(2,1)S(1)}, bf16[2,2,256]{2,1,0:T(2,128)(2,1)S(1)}, u32[]{:S(2)}, u32[]{:S(2)}) collective-permute-start(bf16[2,2,256]{2,1,0:T(2,128)(2,1)S(1)} %pad_maximum_fusion), channel_id=1, source_target_pairs={{0,4},{4,8},{8,12},{12,16},{16,20},{20,24},{24,28},{1,5},{5,9},{9,... | collective-permute-start | bytes 6152 | tf_op jit(solution)/shard_map/ppermute | solution.py:10
  150.0 25.6 %all-to-all-start.1 = ((bf16[8,1,96,512]{3,2,1,0:T(8,128)(2,1)}), bf16[8,1,96,512]{3,2,1,0:T(8,128)(2,1)S(1)}, u32[]{:S(2)}, u32[]{:S(2)}) async-start(bf16[8,1,96,512]{3,2,1,0:T(8,128)(2,1)} %bitcast.116), calls=%async_computation.3 | async-start | bytes 1572864 | tf_op jit(solution)/shard_map/all_to_all | solution.py:71
Sparse Core Ops, SparseCore 0:
  9.5 19.4 all-gather.5
  65.4 26.6 all-gather.3
  112.3 37.7 reduce-scatter.4
  153.0 24.8 reduce-scatter.2
